TPU v7x, 32 devices: a whole 2x2x4 slice. The times are simulated.
32 devices in a mesh: ep: 4 (over y, x), tp: 8 (over z, core).
Axes of the slice: x: 2, y: 2, z: 4, core: 2. Of those that a mesh axis runs over, the one named last changes fastest.
Arguments:
- tokens: bfloat16 [128, 2048], P(('ep', 'tp')), may hold values from -6 to 6
- lengths: int32 [128], P(('ep', 'tp')), may hold values from 64 to 1024
- cache_latent: bfloat16 [128, 1024, 512], P(('ep', 'tp')), may hold values from -6 to 6
- cache_rope_key: bfloat16 [128, 1024, 32], P(('ep', 'tp')), may hold values from -1000 to 1000
- route_ids: int32 [128, 4], P('ep'), may hold values from 0 to 31, all different within a row; in each aligned block of 32 rows (0 to 31, 32 to 63, ...) at most 8 rows name the same one
- route_weights: float32 [128, 4], P('ep'), may hold values from 0.2 to 2
- attn_gain: float32 [2048], replicated, may hold values from 0.1 to 1.9
- w_query_nope: bfloat16 [2048, 16, 64], P(None, 'tp'), may hold values from -0.125 to 0.125
- w_query_rope: bfloat16 [2048, 16, 32], P(None, 'tp'), may hold values from -0.125 to 0.125
- w_latent_down: bfloat16 [2048, 512], P(None, 'tp'), may hold values from -0.125 to 0.125
- w_key_rope: bfloat16 [2048, 32], replicated, may hold values from -0.125 to 0.125
- latent_gain: float32 [512], replicated, may hold values from 0.1 to 1.9
- w_key_up: bfloat16 [512, 16, 64], P(None, 'tp'), may hold values from -0.75 to 0.75
- w_value_up: bfloat16 [512, 16, 64], P(None, 'tp'), may hold values from -0.25 to 0.25
- w_attn_out: bfloat16 [16, 64, 2048], P('tp'), may hold values from -0.1875 to 0.1875
- ffn_gain: float32 [2048], replicated, may hold values from 0.1 to 1.9
- expert_gate: bfloat16 [32, 2048, 512], P(('ep', 'tp')), may hold values from -0.125 to 0.125
- expert_up: bfloat16 [32, 2048, 512], P(('ep', 'tp')), may hold values from -0.125 to 0.125
- expert_down: bfloat16 [32, 512, 2048], P(('ep', 'tp')), may hold values from -0.25 to 0.25
- shared_gate: bfloat16 [2048, 512], P(None, 'tp'), may hold values from -0.125 to 0.125
- shared_up: bfloat16 [2048, 512], P(None, 'tp'), may hold values from -0.125 to 0.125
- shared_down: bfloat16 [512, 2048], P('tp'), may hold values from -0.25 to 0.25
- dense_gate: bfloat16 [2048, 1024], P(None, 'tp'), may hold values from -0.125 to 0.125
- dense_up: bfloat16 [2048, 1024], P(None, 'tp'), may hold values from -0.125 to 0.125
- dense_down: bfloat16 [1024, 2048], P('tp'), may hold values from -0.1875 to 0.1875
- branch_gate: bfloat16 [2048], replicated, may hold values from -0.125 to 0.125
Outputs:
- mixed: bfloat16 [128, 2048], P(('ep', 'tp'))
- new_latent: bfloat16 [128, 512], P(('ep', 'tp'))
- new_rope_key: bfloat16 [128, 32], P(('ep', 'tp'))
Inputs may be any that keep to these rules, and one draw needn't show every extreme that they name: `route_ids`: in each aligned block of 32 rows, no expert is named by more than 8 of the block's rows, a bound that some block reaches. Each row names 4 different experts.
All inputs are finite; a program needn't handle non-finite values.
Results may differ from a plain program's by a relative error of at most 0.025.
Values may be sent and summed in bfloat16 or wider, within the bound.
A program may use at most 64 MiB of HBM per device.

v0:
```python
import jax
import jax.numpy as jnp
from jax import lax
from jax.sharding import PartitionSpec as P

epsilon = 1e-06
rope_base = 10000.0


def norm_rows(values, scales):
    values = values.astype(jnp.float32)
    factor = lax.rsqrt(jnp.mean(values * values, axis=-1, keepdims=True) + epsilon)
    return values * factor * scales


def rotate(values, positions):
    half_dim = values.shape[-1] // 2
    frequencies = rope_base ** (-jnp.arange(half_dim).astype(jnp.float32) / half_dim)
    angles = positions.astype(jnp.float32)[:, None] * frequencies[None, :]
    bcast_shape = (angles.shape[0],) + (1,) * (values.ndim - 2) + (half_dim,)
    cosine = jnp.cos(angles).reshape(bcast_shape)
    sine_val = jnp.sin(angles).reshape(bcast_shape)
    first_half = values[..., :half_dim].astype(jnp.float32)
    second_half = values[..., half_dim:].astype(jnp.float32)
    return jnp.concatenate(
        [
            first_half * cosine - second_half * sine_val,
            first_half * sine_val + second_half * cosine,
        ],
        axis=-1,
    )


def swiglu(inputs, gate_w, up_w):
    gate_val = jnp.dot(inputs, gate_w, preferred_element_type=jnp.float32)
    up_val = jnp.dot(inputs, up_w, preferred_element_type=jnp.float32)
    return (jax.nn.silu(gate_val) * up_val).astype(jnp.bfloat16)


def local(
    tokens,
    lengths,
    cache_latent,
    cache_rope_key,
    route_ids,
    route_weights,
    attn_gain,
    w_query_nope,
    w_query_rope,
    w_latent_down,
    w_key_rope,
    latent_gain,
    w_key_up,
    w_value_up,
    w_attn_out,
    ffn_gain,
    expert_gate,
    expert_up,
    expert_down,
    shared_gate,
    shared_up,
    shared_down,
    dense_gate,
    dense_up,
    dense_down,
    branch_gate,
):
    own_rows, model_width = tokens.shape
    tp_count = lax.axis_size("tp")
    ep_count = lax.axis_size("ep")
    tp_index = lax.axis_index("tp")
    local_heads = w_query_nope.shape[1]
    head_scale = (w_query_nope.shape[2] + w_query_rope.shape[2]) ** (-0.5)
    normed = norm_rows(tokens, attn_gain).astype(jnp.bfloat16)
    group_in = lax.all_gather(normed, "tp", axis=0, tiled=True)
    group_rows = group_in.shape[0]
    query_nope = jnp.dot(
        group_in, w_query_nope.reshape(model_width, -1), preferred_element_type=jnp.float32
    )
    query_nope = query_nope.astype(jnp.bfloat16).reshape(group_rows, local_heads, -1)
    query_latent = jnp.einsum(
        "ghn,rhn->ghr", query_nope, w_key_up, preferred_element_type=jnp.float32
    ).astype(jnp.bfloat16)
    query_rope = jnp.dot(
        group_in, w_query_rope.reshape(model_width, -1), preferred_element_type=jnp.float32
    )
    query_rope = query_rope.astype(jnp.bfloat16).reshape(group_rows, local_heads, -1)
    latent_part = jnp.dot(group_in, w_latent_down, preferred_element_type=jnp.float32).astype(
        jnp.bfloat16
    )
    own_latent_q, own_rope_q, latent_raw = (
        lax.all_to_all(query_latent, "tp", split_axis=0, concat_axis=1, tiled=True),
        lax.all_to_all(query_rope, "tp", split_axis=0, concat_axis=1, tiled=True),
        lax.all_to_all(latent_part, "tp", split_axis=0, concat_axis=1, tiled=True),
    )
    new_latent = norm_rows(latent_raw, latent_gain).astype(jnp.bfloat16)
    key_rope = jnp.dot(normed, w_key_rope, preferred_element_type=jnp.float32)
    new_rope = rotate(key_rope, lengths).astype(jnp.bfloat16)
    query_rot = rotate(own_rope_q, lengths).astype(jnp.bfloat16)
    scores = jnp.einsum(
        "bhr,blr->bhl", own_latent_q, cache_latent, preferred_element_type=jnp.float32
    )
    scores = scores + jnp.einsum(
        "bhe,ble->bhl", query_rot, cache_rope_key, preferred_element_type=jnp.float32
    )
    scores = scores * head_scale
    in_range = (
        jnp.arange(cache_latent.shape[1], dtype=jnp.int32)[None, None, :] < lengths[:, None, None]
    )
    scores = jnp.where(in_range, scores, -jnp.inf)
    own_score = jnp.einsum(
        "bhr,br->bh", own_latent_q, new_latent, preferred_element_type=jnp.float32
    )
    own_score = (
        own_score
        + jnp.einsum("bhe,be->bh", query_rot, new_rope, preferred_element_type=jnp.float32)
    ) * head_scale
    peak_score = jnp.maximum(jnp.max(scores, axis=-1), own_score)
    past_exp = jnp.exp(scores - peak_score[..., None])
    own_exp = jnp.exp(own_score - peak_score)
    total_exp = jnp.sum(past_exp, axis=-1) + own_exp
    past_weight = (past_exp / total_exp[..., None]).astype(jnp.bfloat16)
    own_weight = (own_exp / total_exp).astype(jnp.bfloat16)
    out_latent = jnp.einsum(
        "bhl,blr->bhr", past_weight, cache_latent, preferred_element_type=jnp.float32
    )
    out_latent = (
        out_latent
        + own_weight.astype(jnp.float32)[..., None] * new_latent.astype(jnp.float32)[:, None, :]
    )
    out_latent = out_latent.astype(jnp.bfloat16)
    head_latent = lax.all_to_all(out_latent, "tp", split_axis=1, concat_axis=0, tiled=True)
    head_values = jnp.einsum(
        "ghr,rhv->ghv", head_latent, w_value_up, preferred_element_type=jnp.float32
    ).astype(jnp.bfloat16)
    attn_part = jnp.dot(
        head_values.reshape(group_rows, -1),
        w_attn_out.reshape(-1, model_width),
        preferred_element_type=jnp.float32,
    )
    own_start = tp_index * own_rows
    placed = lax.dynamic_update_slice_in_dim(
        jnp.zeros((group_rows, model_width), jnp.float32), tokens.astype(jnp.float32), own_start, 0
    )
    group_after = lax.psum((attn_part + placed).astype(jnp.bfloat16), "tp").astype(jnp.float32)
    ffn_in = norm_rows(group_after, ffn_gain).astype(jnp.bfloat16)
    after_attn = lax.dynamic_slice_in_dim(group_after, own_start, own_rows, 0)
    shared_term = jnp.dot(
        swiglu(ffn_in, shared_gate, shared_up), shared_down, preferred_element_type=jnp.float32
    )
    branch_mix = jax.nn.sigmoid(jnp.dot(ffn_in, branch_gate, preferred_element_type=jnp.float32))
    dense_term = branch_mix[:, None] * jnp.dot(
        swiglu(ffn_in, dense_gate, dense_up), dense_down, preferred_element_type=jnp.float32
    )
    top_count = route_ids.shape[1]
    expert_local = expert_gate.shape[0]
    capacity = max(
        2, (2 * own_rows * top_count + expert_local * ep_count - 1) // (expert_local * ep_count)
    )
    target_count = ep_count * expert_local
    slot_count = target_count * capacity
    column = route_ids // expert_local % tp_count
    target = route_ids // (expert_local * tp_count) * expert_local + route_ids % expert_local
    flat_target = jnp.where(column == tp_index, target, -1).reshape(-1)
    target_hits = (
        flat_target[:, None] == jnp.arange(target_count, dtype=jnp.int32)[None, :]
    ).astype(jnp.int32)
    earlier = jnp.cumsum(target_hits, axis=0) - target_hits
    rank_in = jnp.sum(earlier * target_hits, axis=1)
    slot_index = jnp.where(flat_target >= 0, flat_target * capacity + rank_in, -1).reshape(
        group_rows, top_count
    )
    slot_match = slot_index[:, :, None] == jnp.arange(slot_count, dtype=jnp.int32)[None, None, :]
    dispatch = jnp.any(slot_match, axis=1).astype(jnp.bfloat16)
    combine = jnp.sum(jnp.where(slot_match, route_weights[:, :, None], 0.0), axis=1)
    outgoing = jnp.einsum("gs,gd->sd", dispatch, ffn_in, preferred_element_type=jnp.float32).astype(
        jnp.bfloat16
    )
    outgoing = outgoing.reshape(ep_count, expert_local, capacity, model_width)
    arrived = lax.all_to_all(outgoing, "ep", split_axis=0, concat_axis=0, tiled=True)
    gate_val = jnp.einsum(
        "sxcd,xdf->sxcf", arrived, expert_gate, preferred_element_type=jnp.float32
    )
    up_val = jnp.einsum("sxcd,xdf->sxcf", arrived, expert_up, preferred_element_type=jnp.float32)
    act_val = (jax.nn.silu(gate_val) * up_val).astype(jnp.bfloat16)
    result = jnp.einsum(
        "sxcf,xfd->sxcd", act_val, expert_down, preferred_element_type=jnp.float32
    ).astype(jnp.bfloat16)
    returned = lax.all_to_all(result, "ep", split_axis=0, concat_axis=0, tiled=True)
    routed = jnp.dot(
        combine,
        returned.reshape(slot_count, model_width).astype(jnp.float32),
        precision=lax.Precision.HIGHEST,
    )
    ffn_total = routed + shared_term + dense_term
    mixed = (
        after_attn
        + lax.psum_scatter(
            ffn_total.astype(jnp.bfloat16), "tp", scatter_dimension=0, tiled=True
        ).astype(jnp.float32)
    ).astype(jnp.bfloat16)
    return (mixed, new_latent, new_rope)


def solution(mesh):
    in_specs = (
        P(("ep", "tp"), None),
        P(("ep", "tp")),
        P(("ep", "tp"), None, None),
        P(("ep", "tp"), None, None),
        P("ep", None),
        P("ep", None),
        P(),
        P(None, "tp", None),
        P(None, "tp", None),
        P(None, "tp"),
        P(),
        P(),
        P(None, "tp", None),
        P(None, "tp", None),
        P("tp", None, None),
        P(),
        P(("ep", "tp"), None, None),
        P(("ep", "tp"), None, None),
        P(("ep", "tp"), None, None),
        P(None, "tp"),
        P(None, "tp"),
        P("tp", None),
        P(None, "tp"),
        P(None, "tp"),
        P("tp", None),
        P(),
    )
    out_specs = (P(("ep", "tp"), None), P(("ep", "tp"), None), P(("ep", "tp"), None))
    return jax.shard_map(local, mesh=mesh, in_specs=in_specs, out_specs=out_specs, check_vma=False)
```

profile of v0, /device:TPU:0, one launch (start us, length us, event | category | flops | bytes accessed | tf_op | source)
XLA Modules:
  0.0 222.2 jit_solution(12282794214563576408)
XLA Ops:
  7.2 1.0 fusion.58
  8.2 0.8 fusion.95
  9.1 15.7 %all-gather = bf16[8,4,2048]{2,1,0:T(4,128)(2,1)S(1)} all-gather(bf16[1,4,2048]{2,1,0:T(4,128)(2,1)S(1)} %fusion.95), channel_id=1, replica_groups=mesh['ep'=4,'tp'=8] {'tp'}, dimensions={0}, use_global_device_ids=true | all-gather | bytes 147456 | tf_op jit(solution)/shard_map/all_gather | solution.py:75
  24.8 1.1 convolution_convert_fusion.5
  26.0 0.7 reshape.224
  26.7 4.6 %all-to-all-start.2 = ((bf16[8,2,128]{2,1,0:T(2,128)(2,1)}), bf16[8,2,128]{2,1,0:T(2,128)(2,1)S(1)}, u32[]{:S(2)}, u32[]{:S(2)}) async-start(bf16[8,2,128]{2,1,0:T(2,128)(2,1)} %reshape.224), calls=%async_computation.2 | async-start | bytes 8192 | tf_op jit(solution)/shard_map/all_to_all | solution.py:94
  31.3 0.7 convert_element_type.145
  31.9 0.7 iota_compare_fusion.2
  32.7 1.1 fusion.93
  33.8 0.8 copy.71
  34.6 0.1 eq.39
  34.7 0.1 fusion.53
  34.8 0.2 reduce_window_sum.11
  35.0 0.2 select_reduce_fusion.1
  35.1 0.1 reduce_sum.60
  35.3 1.1 convolution_convert_fusion.6
  36.4 1.3 convolution_convert_fusion.4
  37.8 0.1 reshape.198
  37.9 0.1 fusion.12
  38.0 0.1 subtract_convert_fusion
  38.2 0.6 reshape.219
  38.9 0.1 reshape.200
  39.0 0.7 reshape.222
  39.7 0.7 copy.64
  40.4 0.6 dynamic-slice.1
  41.6 5.1 %all-to-all-start.1 = ((bf16[8,2,128]{2,1,0:T(2,128)(2,1)}), bf16[8,2,128]{2,1,0:T(2,128)(2,1)S(1)}, u32[]{:S(2)}, u32[]{:S(2)}) async-start(bf16[8,2,128]{2,1,0:T(2,128)(2,1)} %reshape.222), calls=%async_computation.1 | async-start | bytes 8192 | tf_op jit(solution)/shard_map/all_to_all | solution.py:93
  46.7 0.1 reshape.225
  46.8 0.1 fusion.63
  47.0 5.2 %all-to-all-done.1 = bf16[8,2,128]{2,1,0:T(2,128)(2,1)S(1)} async-done(((bf16[8,2,128]{2,1,0:T(2,128)(2,1)}), bf16[8,2,128]{2,1,0:T(2,128)(2,1)S(1)}, u32[]{:S(2)}, u32[]{:S(2)}) %all-to-all-start.1) | async-done | bytes 4128 | tf_op jit(solution)/shard_map/all_to_all | solution.py:93
  52.2 3.3 %all-to-all-start = ((bf16[32,2,512]{2,1,0:T(2,128)(2,1)}), bf16[32,2,512]{2,1,0:T(2,128)(2,1)S(1)}, u32[]{:S(2)}, u32[]{:S(2)}) async-start(bf16[32,2,512]{2,1,0:T(2,128)(2,1)} %copy.64), calls=%async_computation | async-start | bytes 131072 | tf_op jit(solution)/shard_map/all_to_all | solution.py:92
  55.6 0.1 reshape.223
  55.8 0.1 fusion.55
  55.9 0.2 fusion.83
  56.0 5.4 %all-to-all-done = bf16[32,2,512]{2,1,0:T(2,128)(2,1)S(1)} async-done(((bf16[32,2,512]{2,1,0:T(2,128)(2,1)}), bf16[32,2,512]{2,1,0:T(2,128)(2,1)S(1)}, u32[]{:S(2)}, u32[]{:S(2)}) %all-to-all-start) | async-done | bytes 65568 | tf_op jit(solution)/shard_map/all_to_all | solution.py:92
  61.5 0.1 fusion.79
  61.7 3.5 %fusion.100 = f32[4,16,1024]{2,1,0:T(8,128)S(1)} fusion(bf16[4,16,512]{2,1,0:T(8,128)(2,1)S(1)} %all_to_all.58, bf16[4,1024,512]{2,1,0:T(8,128)(2,1)} %param.28), kind=kOutput, calls=%fused_computation.141 | convolution fusion | flops 67108864 | bytes 4521984 | tf_op jit(solution)/shard_map/bhr,blr->bhl/dot_general | solution.py:100
  65.2 0.3 fusion.99
  65.5 0.2 fusion.37
  65.8 0.7 fusion.11
  66.5 0.7 copy.68
  67.2 3.3 %all-to-all-start.3 = ((bf16[4,16,512]{2,0,1:T(4,128)(2,1)}), bf16[4,16,512]{2,0,1:T(4,128)(2,1)S(1)}, u32[]{:S(2)}, u32[]{:S(2)}) async-start(bf16[4,16,512]{2,0,1:T(4,128)(2,1)} %copy.68), calls=%async_computation.3 | async-start | bytes 131072 | tf_op jit(solution)/shard_map/all_to_all | solution.py:132
  70.6 0.7 select_reduce_fusion
  71.3 5.1 %all-to-all-done.3 = bf16[4,16,512]{2,0,1:T(4,128)(2,1)S(1)} async-done(((bf16[4,16,512]{2,0,1:T(4,128)(2,1)}), bf16[4,16,512]{2,0,1:T(4,128)(2,1)S(1)}, u32[]{:S(2)}, u32[]{:S(2)}) %all-to-all-start.3) | async-done | bytes 65568 | tf_op jit(solution)/shard_map/all_to_all | solution.py:132
  76.5 1.3 convolution_bitcast_fusion
  77.8 0.7 convert_element_type.161
  78.5 0.1 fusion.52
  78.6 53.5 %all-reduce.4.cloned.1.call-done = bf16[32,2048]{1,0:T(8,128)(2,1)} async-done(((bf16[32,2048]{1,0:T(8,128)(2,1)}), bf16[32,2048]{1,0:T(8,128)(2,1)}) %all-reduce.4.cloned.1.call-update) | async-done | bytes 131088 | tf_op jit(solution)/shard_map/psum | solution.py:145
  132.1 1.0 multiply_reduce_fusion
  133.2 1.8 fusion.2
  135.0 3.6 %all-to-all-start.4 = ((bf16[4,1,8,2048]{3,2,1,0:T(8,128)(2,1)}), bf16[4,1,8,2048]{3,2,1,0:T(8,128)(2,1)S(1)}, u32[]{:S(2)}, u32[]{:S(2)}) async-start(bf16[4,1,8,2048]{3,2,1,0:T(8,128)(2,1)} %fusion.2), calls=%async_computation.4 | async-start | bytes 262144 | tf_op jit(solution)/shard_map/all_to_all | solution.py:180
  138.6 1.8 fusion.96
  140.4 1.9 fusion.97
  142.3 1.4 all-to-all-done.4
  143.7 2.0 fusion.13
  145.7 3.2 %fusion.3 = bf16[4,1,8,2048]{3,2,1,0:T(8,128)(2,1)} fusion(bf16[1,512,2048]{2,1,0:T(8,128)(2,1)S(1)} %copy-done, bf16[1,2048,512]{2,1,0:T(8,128)(2,1)} %param.43, bf16[4,1,8,2048]{3,2,1,0:T(8,128)(2,1)S(1)} %all-to-all-done.4, f32[4,1,8,512]{3,2,0,1:T(8,128)S(1)} %fusion.13), kind=kOutput, calls=%fused_computation.8 | convolution fusion | flops 134381568 | bytes 4521984 | tf_op jit(solution)/shard_map/sxcf,xfd->sxcd/dot_general | solution.py:186
  148.9 3.5 %all-to-all-start.5 = ((bf16[4,1,8,2048]{3,2,1,0:T(8,128)(2,1)}), bf16[4,1,8,2048]{3,2,1,0:T(8,128)(2,1)S(1)}, u32[]{:S(2)}, u32[]{:S(2)}) async-start(bf16[4,1,8,2048]{3,2,1,0:T(8,128)(2,1)} %fusion.3), calls=%async_computation.5 | async-start | bytes 262144 | tf_op jit(solution)/shard_map/all_to_all | solution.py:189
  152.5 0.7 fusion.34
  153.2 4.2 %all-to-all-done.5 = bf16[4,1,8,2048]{3,2,1,0:T(8,128)(2,1)S(1)} async-done(((bf16[4,1,8,2048]{3,2,1,0:T(8,128)(2,1)}), bf16[4,1,8,2048]{3,2,1,0:T(8,128)(2,1)S(1)}, u32[]{:S(2)}, u32[]{:S(2)}) %all-to-all-start.5) | async-done | bytes 131104 | tf_op jit(solution)/shard_map/all_to_all | solution.py:189
  157.4 0.2 fusion.38
  157.6 1.4 convolution_add_fusion
  159.1 2.2 fusion.1
  161.3 1.3 pad_maximum_fusion.3
  162.6 51.4 %all-reduce.6.cloned.1.call-done = bf16[32,2048]{1,0:T(8,128)(2,1)} async-done(((bf16[32,2048]{1,0:T(8,128)(2,1)}), bf16[32,2048]{1,0:T(8,128)(2,1)}) %all-reduce.6.cloned.1.call-update) | async-done | bytes 131088
  214.0 1.4 add_convert_fusion
  (64 shorter events, 0.9 us)
Async XLA Ops:
  7.2 138.5 %copy-start = (bf16[1,512,2048]{2,1,0:T(8,128)(2,1)S(1)}, bf16[1,512,2048]{2,1,0:T(8,128)(2,1)}, u32[]{:S(2)}) copy-start(bf16[1,512,2048]{2,1,0:T(8,128)(2,1)} %param.44) | copy-start | bytes 6291460
  7.2 33.2 %copy-start.18 = (u32[32]{0:T(128)S(1)}, u32[32]{0:T(128)}, u32[]{:S(2)}) copy-start(u32[32]{0:T(128)} %constant.109) | copy-start | bytes 388
  7.2 30.7 %copy-start.10 = (bf16[512,2,64]{0,2,1:T(8,128)(2,1)S(1)}, bf16[512,2,64]{0,2,1:T(8,128)(2,1)}, u32[]{:S(2)}) copy-start(bf16[512,2,64]{0,2,1:T(8,128)(2,1)} %param.38) | copy-start | bytes 393220
  7.2 31.0 %copy-start.14 = (bf16[2048]{0:T(1024)(128)(2,1)S(1)}, bf16[2048]{0:T(1024)(128)(2,1)}, u32[]{:S(2)}) copy-start(bf16[2048]{0:T(1024)(128)(2,1)} %param.51) | copy-start | bytes 12292
  7.2 48.5 %copy-start.16 = (f32[512]{0:T(512)S(1)}, f32[512]{0:T(512)}, u32[]{:S(2)}) copy-start(f32[512]{0:T(512)} %param.37) | copy-start | bytes 6148
  26.7 14.9 %all-to-all-start.2 = ((bf16[8,2,128]{2,1,0:T(2,128)(2,1)}), bf16[8,2,128]{2,1,0:T(2,128)(2,1)S(1)}, u32[]{:S(2)}, u32[]{:S(2)}) async-start(bf16[8,2,128]{2,1,0:T(2,128)(2,1)} %reshape.224), calls=%async_computation.2 | async-start | bytes 8192 | tf_op jit(solution)/shard_map/all_to_all | solution.py:94
  38.1 23.3 %copy-start.12 = (bf16[4,16]{1,0:T(4,128)(2,1)}, bf16[4,16]{1,0:T(4,128)(2,1)S(1)}, u32[]{:S(2)}) copy-start(bf16[4,16]{1,0:T(4,128)(2,1)S(1)} %get-tuple-element.10) | copy-start | bytes 388
  41.6 10.6 %all-to-all-start.1 = ((bf16[8,2,128]{2,1,0:T(2,128)(2,1)}), bf16[8,2,128]{2,1,0:T(2,128)(2,1)S(1)}, u32[]{:S(2)}, u32[]{:S(2)}) async-start(bf16[8,2,128]{2,1,0:T(2,128)(2,1)} %reshape.222), calls=%async_computation.1 | async-start | bytes 8192 | tf_op jit(solution)/shard_map/all_to_all | solution.py:93
  52.2 9.2 %all-to-all-start = ((bf16[32,2,512]{2,1,0:T(2,128)(2,1)}), bf16[32,2,512]{2,1,0:T(2,128)(2,1)S(1)}, u32[]{:S(2)}, u32[]{:S(2)}) async-start(bf16[32,2,512]{2,1,0:T(2,128)(2,1)} %copy.64), calls=%async_computation | async-start | bytes 131072 | tf_op jit(solution)/shard_map/all_to_all | solution.py:92
  55.8 9.4 %copy-start.15 = (bf16[4,512]{1,0:T(4,128)(2,1)}, bf16[4,512]{1,0:T(4,128)(2,1)S(1)}, u32[]{:S(2)}) copy-start(bf16[4,512]{1,0:T(4,128)(2,1)S(1)} %get-tuple-element.4) | copy-start | bytes 12292
  61.6 3.5 %copy-start.6 = (bf16[4,1024,32]{1,2,0:T(8,128)(2,1)S(1)}, bf16[4,1024,32]{1,2,0:T(8,128)(2,1)}, u32[]{:S(2)}) copy-start(bf16[4,1024,32]{1,2,0:T(8,128)(2,1)} %param.29) | copy-start | bytes 786436
  61.6 4.1 %copy-start.1 = (bf16[4,1024,512]{2,1,0:T(8,128)(2,1)S(1)}, bf16[4,1024,512]{2,1,0:T(8,128)(2,1)}, u32[]{:S(2)}) copy-start(bf16[4,1024,512]{2,1,0:T(8,128)(2,1)} %param.28) | copy-start | bytes 12582916
  65.8 4.8 %copy-start.17 = (f32[32,4]{0,1:T(4,128)S(1)}, f32[32,4]{0,1:T(4,128)}, u32[]{:S(2)}) copy-start(f32[32,4]{0,1:T(4,128)} %param.31) | copy-start | bytes 1540
  65.8 10.7 %copy-start.4 = (bf16[2,64,2048]{2,1,0:T(8,128)(2,1)S(1)}, bf16[2,64,2048]{2,1,0:T(8,128)(2,1)}, u32[]{:S(2)}) copy-start(bf16[2,64,2048]{2,1,0:T(8,128)(2,1)} %param.40) | copy-start | bytes 1572868
  65.8 12.0 %copy-start.9 = (bf16[4,2048]{1,0:T(4,128)(2,1)S(1)}, bf16[4,2048]{1,0:T(4,128)(2,1)}, u32[]{:S(2)}) copy-start(bf16[4,2048]{1,0:T(4,128)(2,1)} %param.26) | copy-start | bytes 49156
  66.5 66.7 %copy-start.8 = (f32[2048]{0:T(1024)S(1)}, f32[2048]{0:T(1024)}, u32[]{:S(2)}) copy-start(f32[2048]{0:T(1024)} %param.41) | copy-start | bytes 24580
  66.5 72.1 %copy-start.3 = (bf16[2048,128]{1,0:T(8,128)(2,1)S(1)}, bf16[2048,128]{1,0:T(8,128)(2,1)}, u32[]{:S(2)}) copy-start(bf16[2048,128]{1,0:T(8,128)(2,1)} %param.48) | copy-start | bytes 1572868
  67.2 9.2 %all-to-all-start.3 = ((bf16[4,16,512]{2,0,1:T(4,128)(2,1)}), bf16[4,16,512]{2,0,1:T(4,128)(2,1)S(1)}, u32[]{:S(2)}, u32[]{:S(2)}) async-start(bf16[4,16,512]{2,0,1:T(4,128)(2,1)} %copy.68), calls=%async_computation.3 | async-start | bytes 131072 | tf_op jit(solution)/shard_map/all_to_all | solution.py:132
  70.5 61.6 %all-reduce.4.cloned.1.call-start = ((), (), s32[]{:S(2)}) async-start(), calls=%async_computation.6 | async-start | bytes 262144 | tf_op jit(solution)/shard_map/psum | solution.py:145
  135.0 8.7 %all-to-all-start.4 = ((bf16[4,1,8,2048]{3,2,1,0:T(8,128)(2,1)}), bf16[4,1,8,2048]{3,2,1,0:T(8,128)(2,1)S(1)}, u32[]{:S(2)}, u32[]{:S(2)}) async-start(bf16[4,1,8,2048]{3,2,1,0:T(8,128)(2,1)} %fusion.2), calls=%async_computation.4 | async-start | bytes 262144 | tf_op jit(solution)/shard_map/all_to_all | solution.py:180
  145.7 6.7 %copy-start.2 = (bf16[32,2048]{1,0:T(8,128)(2,1)S(1)}, bf16[32,2048]{1,0:T(8,128)(2,1)}, u32[]{:S(2)}) copy-start(bf16[32,2048]{1,0:T(8,128)(2,1)} %all-reduce.4.cloned.1.call-done) | copy-start | bytes 393220
  145.7 6.7 %copy-start.13 = (bf16[2048,1]{0,1:T(2,128)(2,1)S(1)}, bf16[2048,1]{0,1:T(2,128)(2,1)}, u32[]{:S(2)}) copy-start(bf16[2048,1]{0,1:T(2,128)(2,1)} %reshape.219) | copy-start | bytes 12292
  145.7 11.7 %copy-start.11 = (f32[32,32]{1,0:T(8,128)S(1)}, f32[32,32]{1,0:T(8,128)}, u32[]{:S(2)}) copy-start(f32[32,32]{1,0:T(8,128)} %select_reduce_fusion) | copy-start | bytes 12292
  145.7 11.9 %copy-start.7 = (bf16[64,2048]{1,0:T(8,128)(2,1)S(1)}, bf16[64,2048]{1,0:T(8,128)(2,1)}, u32[]{:S(2)}) copy-start(bf16[64,2048]{1,0:T(8,128)(2,1)} %param.47) | copy-start | bytes 786436
  148.9 10.2 %copy-start.5 = (bf16[128,2048]{1,0:T(8,128)(2,1)S(1)}, bf16[128,2048]{1,0:T(8,128)(2,1)}, u32[]{:S(2)}) copy-start(bf16[128,2048]{1,0:T(8,128)(2,1)} %param.50) | copy-start | bytes 1572868
  148.9 8.4 %all-to-all-start.5 = ((bf16[4,1,8,2048]{3,2,1,0:T(8,128)(2,1)}), bf16[4,1,8,2048]{3,2,1,0:T(8,128)(2,1)S(1)}, u32[]{:S(2)}, u32[]{:S(2)}) async-start(bf16[4,1,8,2048]{3,2,1,0:T(8,128)(2,1)} %fusion.3), calls=%async_computation.5 | async-start | bytes 262144 | tf_op jit(solution)/shard_map/all_to_all | solution.py:189
  152.4 61.6 %all-reduce.6.cloned.1.call-start = ((), (), s32[]{:S(2)}) async-start(), calls=%async_computation.7 | async-start | bytes 262144
Sparse Core Ops, SparseCore 0:
  78.6 53.4 all-reduce.3
  161.4 52.5 all-reduce.5
where the time goes:
time: 223 us; the launch traced here: 222 us
  waiting for transfers between devices  126 us (57%)
  matrix products  26.3 us (12%)
  starting transfers between devices  23.6 us (11%)
  blocking collectives  15.7 us (7%)
  between operations  15.1 us (7%)
  other arithmetic  9.66 us (4%)
  local copies, waits for them, and re-layouts  5.69 us (3%)
    psum x1, waiting for transfers between devices, local(): lax.psum((attn_part + placed).astype(jnp.bfloat16), 'tp')  53.5 us
    unnamed x3, waiting for transfers between devices  51.4 us
    all_gather x1, blocking collectives, local(): group_in = lax.all_gather(normed, 'tp', axis=0, tiled=True)  15.7 us
    all_to_all x1, waiting for transfers between devices, local(): lax.all_to_all(query_latent, 'tp', split_axis=0, concat_axis=1, tiled=True)  5.38 us
    all_to_all x1, waiting for transfers between devices, local(): lax.all_to_all(query_rope, 'tp', split_axis=0, concat_axis=1, tiled=True)  5.2 us
    all_to_all x1, starting transfers between devices, local(): lax.all_to_all(query_rope, 'tp', split_axis=0, concat_axis=1, tiled=True)  5.11 us
    all_to_all x1, waiting for transfers between devices, local(): lax.all_to_all(out_latent, 'tp', split_axis=1, concat_axis=0, tiled=True)  5.08 us
    all_to_all x1, starting transfers between devices, local(): lax.all_to_all(latent_part, 'tp', split_axis=0, concat_axis=1, tiled=True)  4.6 us
  transfers between devices with their start and end apart: 8, of which 7 were waited for; matrix products, arithmetic and copies ran while one was open for 8% of the time, Pallas kernels for 0%

commit v1 on v0

--- a/solution.py
+++ b/solution.py
@@ -72,7 +72,12 @@
     local_heads = w_query_nope.shape[1]
     head_scale = (w_query_nope.shape[2] + w_query_rope.shape[2]) ** (-0.5)
     normed = norm_rows(tokens, attn_gain).astype(jnp.bfloat16)
-    group_in = lax.all_gather(normed, "tp", axis=0, tiled=True)
+    ring = [normed]
+    for hop in range(7):
+        ring.append(lax.ppermute(ring[-1], "tp", [(dev, (dev + 1) % 8) for dev in range(8)]))
+    group_in = jnp.roll(
+        jnp.concatenate(ring[::-1], axis=0), (lax.axis_index("tp") + 1) * ring[0].shape[0], axis=0
+    )
     group_rows = group_in.shape[0]
     query_nope = jnp.dot(
         group_in, w_query_nope.reshape(model_width, -1), preferred_element_type=jnp.float32

time: 223 us -> 237 us (1.063)
  waiting for transfers between devices: 126 us -> 158 us
  blocking collectives: 15.7 us -> 0 us
  starting transfers between devices: 23.6 us -> 21.1 us
    ppermute x0 -> x7, waiting for transfers between devices: none -> 27.8 us  [local(): lax.ppermute(ring[-1], 'tp', [(dev, (dev + 1) % 8) for dev in range(8)])]
    all_gather x1 -> x0, blocking collectives: 15.7 us -> none  [local(): group_in = lax.all_gather(normed, 'tp', axis=0, tiled=True)]
    all_to_all x1, waiting for transfers between devices: 0.01 us -> 3.83 us  [local(): lax.all_to_all(latent_part, 'tp', split_axis=0, concat_axis=1, tiled=True)]
    unnamed x46 -> x43, local copies, waits for them, and re-layouts: 3.64 us -> 4.95 us
  transfers between devices with their start and end apart: 8 -> 15, of which waited for: 7 -> 15; matrix products, arithmetic and copies ran while one was open for 8% -> 7% of each run, Pallas kernels for 0% -> 0%
where the time goes in v1:
time: 237 us; the launch traced here: 236 us
  waiting for transfers between devices  158 us (67%)
  matrix products  25.2 us (11%)
  starting transfers between devices  21.1 us (9%)
  between operations  15.1 us (6%)
  other arithmetic  9.59 us (4%)
  local copies, waits for them, and re-layouts  7.24 us (3%)
    psum x1, waiting for transfers between devices, local(): lax.psum((attn_part + placed).astype(jnp.bfloat16), 'tp')  54 us
    unnamed x3, waiting for transfers between devices  51.4 us
    ppermute x7, waiting for transfers between devices, local(): lax.ppermute(ring[-1], 'tp', [(dev, (dev + 1) % 8) for dev in range(8)])  27.8 us
    all_to_all x1, waiting for transfers between devices, local(): lax.all_to_all(query_latent, 'tp', split_axis=0, concat_axis=1, tiled=True)  5.38 us
    all_to_all x1, waiting for transfers between devices, local(): lax.all_to_all(query_rope, 'tp', split_axis=0, concat_axis=1, tiled=True)  5.13 us
    all_to_all x1, waiting for transfers between devices, local(): lax.all_to_all(out_latent, 'tp', split_axis=1, concat_axis=0, tiled=True)  5.08 us
    unnamed x43, local copies, waits for them, and re-layouts  4.95 us
  transfers between devices with their start and end apart: 15, of which 15 were waited for; matrix products, arithmetic and copies ran while one was open for 7% of the time, Pallas kernels for 0%

profile of v1, /device:TPU:0, one launch (start us, length us, event | category | flops | bytes accessed | tf_op | source)
XLA Modules:
  0.0 236.4 jit_solution(13082891619374500317)
XLA Ops:
  7.2 1.0 fusion.61
  8.2 0.8 fusion.63
  9.0 0.5 collective-permute-start
  9.6 1.0 fusion.104
  10.6 0.8 copy.71
  11.6 0.2 reduce_window_sum.11
  11.8 3.2 %collective-permute-done = bf16[4,2048]{1,0:T(4,128)(2,1)S(1)} collective-permute-done((bf16[4,2048]{1,0:T(4,128)(2,1)S(1)}, bf16[4,2048]{1,0:T(4,128)(2,1)S(1)}, u32[]{:S(2)}, u32[]{:S(2)}) %collective-permute-start) | collective-permute-done | bytes 16416 | tf_op jit(solution)/shard_map/ppermute | solution.py:77
  15.0 0.2 select_reduce_fusion.1
  15.3 4.7 %collective-permute-done.1 = bf16[4,2048]{1,0:T(4,128)(2,1)S(1)} collective-permute-done((bf16[4,2048]{1,0:T(4,128)(2,1)S(1)}, bf16[4,2048]{1,0:T(4,128)(2,1)S(1)}, u32[]{:S(2)}, u32[]{:S(2)}) %collective-permute-start.1) | collective-permute-done | bytes 16416 | tf_op jit(solution)/shard_map/ppermute | solution.py:77
  20.0 4.9 %collective-permute-done.2 = bf16[4,2048]{1,0:T(4,128)(2,1)S(1)} collective-permute-done((bf16[4,2048]{1,0:T(4,128)(2,1)S(1)}, bf16[4,2048]{1,0:T(4,128)(2,1)S(1)}, u32[]{:S(2)}, u32[]{:S(2)}) %collective-permute-start.2) | collective-permute-done | bytes 16416 | tf_op jit(solution)/shard_map/ppermute | solution.py:77
  25.0 0.7 convert_element_type.145
  25.6 4.3 %collective-permute-done.3 = bf16[4,2048]{1,0:T(4,128)(2,1)S(1)} collective-permute-done((bf16[4,2048]{1,0:T(4,128)(2,1)S(1)}, bf16[4,2048]{1,0:T(4,128)(2,1)S(1)}, u32[]{:S(2)}, u32[]{:S(2)}) %collective-permute-start.3) | collective-permute-done | bytes 16416 | tf_op jit(solution)/shard_map/ppermute | solution.py:77
  29.9 0.1 subtract_convert_fusion
  30.0 4.8 %collective-permute-done.4 = bf16[4,2048]{1,0:T(4,128)(2,1)S(1)} collective-permute-done((bf16[4,2048]{1,0:T(4,128)(2,1)S(1)}, bf16[4,2048]{1,0:T(4,128)(2,1)S(1)}, u32[]{:S(2)}, u32[]{:S(2)}) %collective-permute-start.4) | collective-permute-done | bytes 16416 | tf_op jit(solution)/shard_map/ppermute | solution.py:77
  34.9 0.7 iota_compare_fusion.2
  35.6 4.2 %collective-permute-done.5 = bf16[4,2048]{1,0:T(4,128)(2,1)S(1)} collective-permute-done((bf16[4,2048]{1,0:T(4,128)(2,1)S(1)}, bf16[4,2048]{1,0:T(4,128)(2,1)S(1)}, u32[]{:S(2)}, u32[]{:S(2)}) %collective-permute-start.5) | collective-permute-done | bytes 16416 | tf_op jit(solution)/shard_map/ppermute | solution.py:77
  39.9 1.3 reshape.217
  41.3 1.2 dynamic-slice.1
  43.2 1.6 collective-permute-done.6
  44.8 0.3 concatenate.14
  45.1 1.1 convolution_convert_fusion.6
  46.2 1.2 convolution_convert_fusion.5
  47.4 0.3 convolution_convert_fusion.4
  47.7 0.7 reshape.222
  48.4 3.3 %all-to-all-start.2 = ((bf16[8,2,128]{2,1,0:T(2,128)(2,1)}), bf16[8,2,128]{2,1,0:T(2,128)(2,1)S(1)}, u32[]{:S(2)}, u32[]{:S(2)}) async-start(bf16[8,2,128]{2,1,0:T(2,128)(2,1)} %reshape.222), calls=%async_computation.2 | async-start | bytes 8192 | tf_op jit(solution)/shard_map/all_to_all | solution.py:99
  51.8 0.1 fusion.12
  52.0 0.7 reshape.220
  52.7 0.7 copy.64
  53.4 3.8 %all-to-all-done.2 = bf16[8,2,128]{2,1,0:T(2,128)(2,1)S(1)} async-done(((bf16[8,2,128]{2,1,0:T(2,128)(2,1)}), bf16[8,2,128]{2,1,0:T(2,128)(2,1)S(1)}, u32[]{:S(2)}, u32[]{:S(2)}) %all-to-all-start.2) | async-done | bytes 4128 | tf_op jit(solution)/shard_map/all_to_all | solution.py:99
  57.2 3.3 %all-to-all-start.1 = ((bf16[8,2,128]{2,1,0:T(2,128)(2,1)}), bf16[8,2,128]{2,1,0:T(2,128)(2,1)S(1)}, u32[]{:S(2)}, u32[]{:S(2)}) async-start(bf16[8,2,128]{2,1,0:T(2,128)(2,1)} %reshape.220), calls=%async_computation.1 | async-start | bytes 8192 | tf_op jit(solution)/shard_map/all_to_all | solution.py:98
  60.6 0.1 fusion.66
  60.9 5.1 %all-to-all-done.1 = bf16[8,2,128]{2,1,0:T(2,128)(2,1)S(1)} async-done(((bf16[8,2,128]{2,1,0:T(2,128)(2,1)}), bf16[8,2,128]{2,1,0:T(2,128)(2,1)S(1)}, u32[]{:S(2)}, u32[]{:S(2)}) %all-to-all-start.1) | async-done | bytes 4128 | tf_op jit(solution)/shard_map/all_to_all | solution.py:98
  66.0 3.3 %all-to-all-start = ((bf16[32,2,512]{2,1,0:T(2,128)(2,1)}), bf16[32,2,512]{2,1,0:T(2,128)(2,1)S(1)}, u32[]{:S(2)}, u32[]{:S(2)}) async-start(bf16[32,2,512]{2,1,0:T(2,128)(2,1)} %copy.64), calls=%async_computation | async-start | bytes 131072 | tf_op jit(solution)/shard_map/all_to_all | solution.py:97
  69.6 0.2 fusion.86
  69.8 5.4 %all-to-all-done = bf16[32,2,512]{2,1,0:T(2,128)(2,1)S(1)} async-done(((bf16[32,2,512]{2,1,0:T(2,128)(2,1)}), bf16[32,2,512]{2,1,0:T(2,128)(2,1)S(1)}, u32[]{:S(2)}, u32[]{:S(2)}) %all-to-all-start) | async-done | bytes 65568 | tf_op jit(solution)/shard_map/all_to_all | solution.py:97
  75.3 0.1 fusion.82
  75.4 3.5 %fusion.103 = f32[4,16,1024]{2,1,0:T(8,128)S(1)} fusion(bf16[4,16,512]{2,1,0:T(8,128)(2,1)S(1)} %all_to_all.58, bf16[4,1024,512]{2,1,0:T(8,128)(2,1)} %param.28), kind=kOutput, calls=%fused_computation.145 | convolution fusion | flops 67108864 | bytes 4521984 | tf_op jit(solution)/shard_map/bhr,blr->bhl/dot_general | solution.py:105
  78.9 0.3 fusion.102
  79.3 0.2 fusion.37
  79.6 0.7 fusion.11
  80.3 0.7 copy.68
  80.9 3.3 %all-to-all-start.3 = ((bf16[4,16,512]{2,0,1:T(4,128)(2,1)}), bf16[4,16,512]{2,0,1:T(4,128)(2,1)S(1)}, u32[]{:S(2)}, u32[]{:S(2)}) async-start(bf16[4,16,512]{2,0,1:T(4,128)(2,1)} %copy.68), calls=%async_computation.3 | async-start | bytes 131072 | tf_op jit(solution)/shard_map/all_to_all | solution.py:137
  84.4 0.7 select_reduce_fusion
  85.1 5.1 %all-to-all-done.3 = bf16[4,16,512]{2,0,1:T(4,128)(2,1)S(1)} async-done(((bf16[4,16,512]{2,0,1:T(4,128)(2,1)}), bf16[4,16,512]{2,0,1:T(4,128)(2,1)S(1)}, u32[]{:S(2)}, u32[]{:S(2)}) %all-to-all-start.3) | async-done | bytes 65568 | tf_op jit(solution)/shard_map/all_to_all | solution.py:137
  90.2 1.3 convolution_bitcast_fusion
  91.6 0.7 convert_element_type.161
  92.3 54.0 %all-reduce.4.cloned.1.call-done = bf16[32,2048]{1,0:T(8,128)(2,1)} async-done(((bf16[32,2048]{1,0:T(8,128)(2,1)}), bf16[32,2048]{1,0:T(8,128)(2,1)}) %all-reduce.4.cloned.1.call-update) | async-done | bytes 131088 | tf_op jit(solution)/shard_map/psum | solution.py:150
  146.4 1.0 multiply_reduce_fusion
  147.4 1.8 fusion.2
  149.2 3.6 %all-to-all-start.4 = ((bf16[4,1,8,2048]{3,2,1,0:T(8,128)(2,1)}), bf16[4,1,8,2048]{3,2,1,0:T(8,128)(2,1)S(1)}, u32[]{:S(2)}, u32[]{:S(2)}) async-start(bf16[4,1,8,2048]{3,2,1,0:T(8,128)(2,1)} %fusion.2), calls=%async_computation.4 | async-start | bytes 262144 | tf_op jit(solution)/shard_map/all_to_all | solution.py:185
  152.9 1.8 fusion.99
  154.6 1.9 fusion.100
  156.5 1.4 all-to-all-done.4
  157.9 2.0 fusion.13
  160.0 3.2 %fusion.3 = bf16[4,1,8,2048]{3,2,1,0:T(8,128)(2,1)} fusion(bf16[1,512,2048]{2,1,0:T(8,128)(2,1)S(1)} %copy-done, bf16[1,2048,512]{2,1,0:T(8,128)(2,1)} %param.43, bf16[4,1,8,2048]{3,2,1,0:T(8,128)(2,1)S(1)} %all-to-all-done.4, f32[4,1,8,512]{3,2,0,1:T(8,128)S(1)} %fusion.13), kind=kOutput, calls=%fused_computation.8 | convolution fusion | flops 134381568 | bytes 4521984 | tf_op jit(solution)/shard_map/sxcf,xfd->sxcd/dot_general | solution.py:191
  163.2 3.5 %all-to-all-start.5 = ((bf16[4,1,8,2048]{3,2,1,0:T(8,128)(2,1)}), bf16[4,1,8,2048]{3,2,1,0:T(8,128)(2,1)S(1)}, u32[]{:S(2)}, u32[]{:S(2)}) async-start(bf16[4,1,8,2048]{3,2,1,0:T(8,128)(2,1)} %fusion.3), calls=%async_computation.5 | async-start | bytes 262144 | tf_op jit(solution)/shard_map/all_to_all | solution.py:194
  166.7 0.7 fusion.34
  167.4 4.2 %all-to-all-done.5 = bf16[4,1,8,2048]{3,2,1,0:T(8,128)(2,1)S(1)} async-done(((bf16[4,1,8,2048]{3,2,1,0:T(8,128)(2,1)}), bf16[4,1,8,2048]{3,2,1,0:T(8,128)(2,1)S(1)}, u32[]{:S(2)}, u32[]{:S(2)}) %all-to-all-start.5) | async-done | bytes 131104 | tf_op jit(solution)/shard_map/all_to_all | solution.py:194
  171.6 0.2 fusion.38
  171.9 1.4 convolution_add_fusion
  173.3 2.2 fusion.1
  175.5 1.3 pad_maximum_fusion.3
  176.8 51.4 %all-reduce.6.cloned.1.call-done = bf16[32,2048]{1,0:T(8,128)(2,1)} async-done(((bf16[32,2048]{1,0:T(8,128)(2,1)}), bf16[32,2048]{1,0:T(8,128)(2,1)}) %all-reduce.6.cloned.1.call-update) | async-done | bytes 131088
  228.2 1.4 add_convert_fusion
  (75 shorter events, 1.6 us)
Async XLA Ops:
  7.2 152.8 %copy-start = (bf16[1,512,2048]{2,1,0:T(8,128)(2,1)S(1)}, bf16[1,512,2048]{2,1,0:T(8,128)(2,1)}, u32[]{:S(2)}) copy-start(bf16[1,512,2048]{2,1,0:T(8,128)(2,1)} %param.44) | copy-start | bytes 6291460
  7.2 40.2 %copy-start.3 = (bf16[2048,2,64]{0,2,1:T(8,128)(2,1)S(1)}, bf16[2048,2,64]{0,2,1:T(8,128)(2,1)}, u32[]{:S(2)}) copy-start(bf16[2048,2,64]{0,2,1:T(8,128)(2,1)} %param.33) | copy-start | bytes 1572868
  7.2 44.6 %copy-start.11 = (bf16[512,2,64]{0,2,1:T(8,128)(2,1)S(1)}, bf16[512,2,64]{0,2,1:T(8,128)(2,1)}, u32[]{:S(2)}) copy-start(bf16[512,2,64]{0,2,1:T(8,128)(2,1)} %param.38) | copy-start | bytes 393220
  7.2 62.2 %copy-start.16 = (f32[512]{0:T(512)S(1)}, f32[512]{0:T(512)}, u32[]{:S(2)}) copy-start(f32[512]{0:T(512)} %param.37) | copy-start | bytes 6148
  9.0 6.0 %collective-permute-start = (bf16[4,2048]{1,0:T(4,128)(2,1)S(1)}, bf16[4,2048]{1,0:T(4,128)(2,1)S(1)}, u32[]{:S(2)}, u32[]{:S(2)}) collective-permute-start(bf16[4,2048]{1,0:T(4,128)(2,1)S(1)} %fusion.63), channel_id=1, source_target_pairs={{0,1},{1,2},{2,3},{3,4},{4,5},{5,6},{6,7},{7,0},{8,9},{9,10},{10,1... | collective-permute-start | bytes 49160 | tf_op jit(solution)/shard_map/ppermute | solution.py:77
  15.0 5.0 %collective-permute-start.1 = (bf16[4,2048]{1,0:T(4,128)(2,1)S(1)}, bf16[4,2048]{1,0:T(4,128)(2,1)S(1)}, u32[]{:S(2)}, u32[]{:S(2)}) collective-permute-start(bf16[4,2048]{1,0:T(4,128)(2,1)S(1)} %collective-permute-done), channel_id=1, source_target_pairs={{0,1},{1,2},{2,3},{3,4},{4,5},{5,6},{6,7},{7,0},{8,9},{9,10},{10,1... | collective-permute-start | bytes 49160 | tf_op jit(solution)/shard_map/ppermute | solution.py:77
  20.0 5.0 %collective-permute-start.2 = (bf16[4,2048]{1,0:T(4,128)(2,1)S(1)}, bf16[4,2048]{1,0:T(4,128)(2,1)S(1)}, u32[]{:S(2)}, u32[]{:S(2)}) collective-permute-start(bf16[4,2048]{1,0:T(4,128)(2,1)S(1)} %collective-permute-done.1), channel_id=1, source_target_pairs={{0,1},{1,2},{2,3},{3,4},{4,5},{5,6},{6,7},{7,0},{8,9},{9,10},{10,1... | collective-permute-start | bytes 49160 | tf_op jit(solution)/shard_map/ppermute | solution.py:77
  24.9 5.0 %collective-permute-start.3 = (bf16[4,2048]{1,0:T(4,128)(2,1)S(1)}, bf16[4,2048]{1,0:T(4,128)(2,1)S(1)}, u32[]{:S(2)}, u32[]{:S(2)}) collective-permute-start(bf16[4,2048]{1,0:T(4,128)(2,1)S(1)} %collective-permute-done.2), channel_id=1, source_target_pairs={{0,1},{1,2},{2,3},{3,4},{4,5},{5,6},{6,7},{7,0},{8,9},{9,10},{10,1... | collective-permute-start | bytes 49160 | tf_op jit(solution)/shard_map/ppermute | solution.py:77
  29.9 5.0 %collective-permute-start.4 = (bf16[4,2048]{1,0:T(4,128)(2,1)S(1)}, bf16[4,2048]{1,0:T(4,128)(2,1)S(1)}, u32[]{:S(2)}, u32[]{:S(2)}) collective-permute-start(bf16[4,2048]{1,0:T(4,128)(2,1)S(1)} %collective-permute-done.3), channel_id=1, source_target_pairs={{0,1},{1,2},{2,3},{3,4},{4,5},{5,6},{6,7},{7,0},{8,9},{9,10},{10,1... | collective-permute-start | bytes 49160 | tf_op jit(solution)/shard_map/ppermute | solution.py:77
  30.0 18.4 %copy-start.13 = (bf16[4,16]{1,0:T(4,128)(2,1)}, bf16[4,16]{1,0:T(4,128)(2,1)S(1)}, u32[]{:S(2)}) copy-start(bf16[4,16]{1,0:T(4,128)(2,1)S(1)} %get-tuple-element.10) | copy-start | bytes 388
  34.9 5.0 %collective-permute-start.5 = (bf16[4,2048]{1,0:T(4,128)(2,1)S(1)}, bf16[4,2048]{1,0:T(4,128)(2,1)S(1)}, u32[]{:S(2)}, u32[]{:S(2)}) collective-permute-start(bf16[4,2048]{1,0:T(4,128)(2,1)S(1)} %collective-permute-done.4), channel_id=1, source_target_pairs={{0,1},{1,2},{2,3},{3,4},{4,5},{5,6},{6,7},{7,0},{8,9},{9,10},{10,1... | collective-permute-start | bytes 49160 | tf_op jit(solution)/shard_map/ppermute | solution.py:77
  39.8 5.0 %collective-permute-start.6 = (bf16[4,2048]{1,0:T(4,128)(2,1)S(1)}, bf16[4,2048]{1,0:T(4,128)(2,1)S(1)}, u32[]{:S(2)}, u32[]{:S(2)}) collective-permute-start(bf16[4,2048]{1,0:T(4,128)(2,1)S(1)} %collective-permute-done.5), channel_id=1, source_target_pairs={{0,1},{1,2},{2,3},{3,4},{4,5},{5,6},{6,7},{7,0},{8,9},{9,10},{10,1... | collective-permute-start | bytes 49160 | tf_op jit(solution)/shard_map/ppermute | solution.py:77
  48.4 8.8 %all-to-all-start.2 = ((bf16[8,2,128]{2,1,0:T(2,128)(2,1)}), bf16[8,2,128]{2,1,0:T(2,128)(2,1)S(1)}, u32[]{:S(2)}, u32[]{:S(2)}) async-start(bf16[8,2,128]{2,1,0:T(2,128)(2,1)} %reshape.222), calls=%async_computation.2 | async-start | bytes 8192 | tf_op jit(solution)/shard_map/all_to_all | solution.py:99
  57.2 8.8 %all-to-all-start.1 = ((bf16[8,2,128]{2,1,0:T(2,128)(2,1)}), bf16[8,2,128]{2,1,0:T(2,128)(2,1)S(1)}, u32[]{:S(2)}, u32[]{:S(2)}) async-start(bf16[8,2,128]{2,1,0:T(2,128)(2,1)} %reshape.220), calls=%async_computation.1 | async-start | bytes 8192 | tf_op jit(solution)/shard_map/all_to_all | solution.py:98
  66.0 9.2 %all-to-all-start = ((bf16[32,2,512]{2,1,0:T(2,128)(2,1)}), bf16[32,2,512]{2,1,0:T(2,128)(2,1)S(1)}, u32[]{:S(2)}, u32[]{:S(2)}) async-start(bf16[32,2,512]{2,1,0:T(2,128)(2,1)} %copy.64), calls=%async_computation | async-start | bytes 131072 | tf_op jit(solution)/shard_map/all_to_all | solution.py:97
  69.5 9.4 %copy-start.15 = (bf16[4,512]{1,0:T(4,128)(2,1)}, bf16[4,512]{1,0:T(4,128)(2,1)S(1)}, u32[]{:S(2)}) copy-start(bf16[4,512]{1,0:T(4,128)(2,1)S(1)} %get-tuple-element.4) | copy-start | bytes 12292
  75.4 3.5 %copy-start.7 = (bf16[4,1024,32]{1,2,0:T(8,128)(2,1)S(1)}, bf16[4,1024,32]{1,2,0:T(8,128)(2,1)}, u32[]{:S(2)}) copy-start(bf16[4,1024,32]{1,2,0:T(8,128)(2,1)} %param.29) | copy-start | bytes 786436
  75.4 4.1 %copy-start.1 = (bf16[4,1024,512]{2,1,0:T(8,128)(2,1)S(1)}, bf16[4,1024,512]{2,1,0:T(8,128)(2,1)}, u32[]{:S(2)}) copy-start(bf16[4,1024,512]{2,1,0:T(8,128)(2,1)} %param.28) | copy-start | bytes 12582916
  79.5 4.8 %copy-start.17 = (f32[32,4]{0,1:T(4,128)S(1)}, f32[32,4]{0,1:T(4,128)}, u32[]{:S(2)}) copy-start(f32[32,4]{0,1:T(4,128)} %param.31) | copy-start | bytes 1540
  79.5 10.7 %copy-start.5 = (bf16[2,64,2048]{2,1,0:T(8,128)(2,1)S(1)}, bf16[2,64,2048]{2,1,0:T(8,128)(2,1)}, u32[]{:S(2)}) copy-start(bf16[2,64,2048]{2,1,0:T(8,128)(2,1)} %param.40) | copy-start | bytes 1572868
  79.5 12.0 %copy-start.10 = (bf16[4,2048]{1,0:T(4,128)(2,1)S(1)}, bf16[4,2048]{1,0:T(4,128)(2,1)}, u32[]{:S(2)}) copy-start(bf16[4,2048]{1,0:T(4,128)(2,1)} %param.26) | copy-start | bytes 49156
  80.3 67.1 %copy-start.9 = (f32[2048]{0:T(1024)S(1)}, f32[2048]{0:T(1024)}, u32[]{:S(2)}) copy-start(f32[2048]{0:T(1024)} %param.41) | copy-start | bytes 24580
  80.3 72.6 %copy-start.4 = (bf16[2048,128]{1,0:T(8,128)(2,1)S(1)}, bf16[2048,128]{1,0:T(8,128)(2,1)}, u32[]{:S(2)}) copy-start(bf16[2048,128]{1,0:T(8,128)(2,1)} %param.48) | copy-start | bytes 1572868
  80.9 9.2 %all-to-all-start.3 = ((bf16[4,16,512]{2,0,1:T(4,128)(2,1)}), bf16[4,16,512]{2,0,1:T(4,128)(2,1)S(1)}, u32[]{:S(2)}, u32[]{:S(2)}) async-start(bf16[4,16,512]{2,0,1:T(4,128)(2,1)} %copy.68), calls=%async_computation.3 | async-start | bytes 131072 | tf_op jit(solution)/shard_map/all_to_all | solution.py:137
  84.3 62.1 %all-reduce.4.cloned.1.call-start = ((), (), s32[]{:S(2)}) async-start(), calls=%async_computation.6 | async-start | bytes 262144 | tf_op jit(solution)/shard_map/psum | solution.py:150
  149.2 8.7 %all-to-all-start.4 = ((bf16[4,1,8,2048]{3,2,1,0:T(8,128)(2,1)}), bf16[4,1,8,2048]{3,2,1,0:T(8,128)(2,1)S(1)}, u32[]{:S(2)}, u32[]{:S(2)}) async-start(bf16[4,1,8,2048]{3,2,1,0:T(8,128)(2,1)} %fusion.2), calls=%async_computation.4 | async-start | bytes 262144 | tf_op jit(solution)/shard_map/all_to_all | solution.py:185
  159.9 6.7 %copy-start.2 = (bf16[32,2048]{1,0:T(8,128)(2,1)S(1)}, bf16[32,2048]{1,0:T(8,128)(2,1)}, u32[]{:S(2)}) copy-start(bf16[32,2048]{1,0:T(8,128)(2,1)} %all-reduce.4.cloned.1.call-done) | copy-start | bytes 393220
  159.9 6.7 %copy-start.14 = (bf16[2048,1]{0,1:T(2,128)(2,1)S(1)}, bf16[2048,1]{0,1:T(2,128)(2,1)}, u32[]{:S(2)}) copy-start(bf16[2048,1]{0,1:T(2,128)(2,1)} %reshape.217) | copy-start | bytes 12292
  159.9 11.7 %copy-start.12 = (f32[32,32]{1,0:T(8,128)S(1)}, f32[32,32]{1,0:T(8,128)}, u32[]{:S(2)}) copy-start(f32[32,32]{1,0:T(8,128)} %select_reduce_fusion) | copy-start | bytes 12292
  160.0 11.9 %copy-start.8 = (bf16[64,2048]{1,0:T(8,128)(2,1)S(1)}, bf16[64,2048]{1,0:T(8,128)(2,1)}, u32[]{:S(2)}) copy-start(bf16[64,2048]{1,0:T(8,128)(2,1)} %param.47) | copy-start | bytes 786436
  163.2 10.2 %copy-start.6 = (bf16[128,2048]{1,0:T(8,128)(2,1)S(1)}, bf16[128,2048]{1,0:T(8,128)(2,1)}, u32[]{:S(2)}) copy-start(bf16[128,2048]{1,0:T(8,128)(2,1)} %param.50) | copy-start | bytes 1572868
  163.2 8.4 %all-to-all-start.5 = ((bf16[4,1,8,2048]{3,2,1,0:T(8,128)(2,1)}), bf16[4,1,8,2048]{3,2,1,0:T(8,128)(2,1)S(1)}, u32[]{:S(2)}, u32[]{:S(2)}) async-start(bf16[4,1,8,2048]{3,2,1,0:T(8,128)(2,1)} %fusion.3), calls=%async_computation.5 | async-start | bytes 262144 | tf_op jit(solution)/shard_map/all_to_all | solution.py:194
  166.6 61.6 %all-reduce.6.cloned.1.call-start = ((), (), s32[]{:S(2)}) async-start(), calls=%async_computation.7 | async-start | bytes 262144
Sparse Core Ops, SparseCore 0:
  92.4 53.9 all-reduce.3
  175.6 52.5 all-reduce.5
